TPU v7x, 128 devices: a whole 4x4x4 slice. The times are simulated.
128 devices in a mesh: sp: 32 (over z, y, core), tp: 4 (over x).
Axes of the slice: x: 4, y: 4, z: 4, core: 2. Of those that a mesh axis runs over, the one named last changes fastest.
Arguments:
- mixer_value_projection: bfloat16 [24576, 2048], P('sp', 'tp'), may hold values from -6 to 6
- write_vectors_projected: bfloat16 [24576, 256], P('sp', 'tp'), may hold values from -6 to 6
- read_vectors_projected: bfloat16 [24576, 256], P('sp', 'tp'), may hold values from -6 to 6
- output_gate_projected: bfloat16 [24576, 2048], P('sp', 'tp'), may hold values from -6 to 6
- step_size_scores: float32 [24576, 32], P('sp', 'tp'), may hold values from -8 to 8
- position_decay_extra: float32 [24576, 32], P('sp', 'tp'), may hold values from -1 to 0
- step_size_bias: float32 [32], P('tp'), may hold values from -1 to 1
- head_decay_logarithm: float32 [32], P('tp'), may hold values from -14 to -3
- value_filter_taps: bfloat16 [4, 2048], P(None, 'tp'), may hold values from -3 to 3
- write_filter_taps: bfloat16 [4, 256], P(None, 'tp'), may hold values from -3 to 3
- read_filter_taps: bfloat16 [4, 256], P(None, 'tp'), may hold values from -3 to 3
- gated_group_norm_gain: float32 [2048], P('tp'), may hold values from 0.1 to 1.9
- mixer_output_weight: bfloat16 [2048, 2048], P('tp'), may hold values from -0.125 to 0.125
- residual: bfloat16 [24576, 2048], P('sp'), may hold values from -6 to 6
- feedforward_norm_gain: float32 [2048], replicated, may hold values from 0.1 to 1.9
- feedforward_gate_weight: bfloat16 [2048, 5632], P('sp', 'tp'), may hold values from -0.125 to 0.125
- feedforward_value_weight: bfloat16 [2048, 5632], P('sp', 'tp'), may hold values from -0.125 to 0.125
- gate_filter_taps: bfloat16 [3, 5632], P(None, 'tp'), may hold values from -3.5 to 3.5
- single_value_filter_taps: bfloat16 [3, 5632], P(None, 'tp'), may hold values from -3.5 to 3.5
- feedforward_down_weight: bfloat16 [5632, 2048], P('tp', 'sp'), may hold values from -0.078125 to 0.078125
Outputs:
- mixed: bfloat16 [24576, 2048], P(('sp', 'tp'))
All inputs are finite; a program needn't handle non-finite values.
Results may differ from a plain program's by a relative error of at most 0.012.
Values may be sent and summed in bfloat16 or wider, within the bound.
No kernel may reach another device: no remote copies, remote signals or barrier semaphores. Data moves between devices by JAX's collectives and lax.ppermute only.
A program may use at most 192 MiB of HBM per device.

v0:
```python
import jax
import jax.numpy as jnp
from jax import lax
from jax.sharding import Mesh
from jax.sharding import PartitionSpec as P

HEAD = 64
STATE = 64
BLOCK = 128
SP = ("sp_0", "sp_1", "sp_2")
SP_TP = ("sp_0", "sp_1", "sp_2", "tp")


epsilon = 1e-06


def from_behind(value, axis, by):
    length = lax.axis_size(axis)
    pairs = [(i, i + by) for i in range(length) if 0 <= i + by < length]
    return lax.ppermute(value, axis, pairs)


def nothing_yet(value, identity):
    return jax.tree.map(
        lambda part, zero: jnp.zeros_like(part) + jnp.asarray(zero, part.dtype), value, identity
    )


def entering_2(value, axes, combine, identity):
    before = start = nothing_yet(value, identity)
    running = value
    for axis in reversed(axes):
        length, here = (lax.axis_size(axis), lax.axis_index(axis))
        pieces = jax.tree.map(lambda part: lax.all_gather(part, axis), running)
        inside, running = (start, start)
        for k in range(length):
            passed = k < here
            running = combine(running, jax.tree.map(lambda part: part[k], pieces))
            inside = jax.tree.map(lambda new, old: jnp.where(passed, new, old), running, inside)
        before = combine(inside, before)
    return before


def in_order(parts, dim):
    lengths = list(parts.shape[1:])
    lengths[dim] *= parts.shape[0]
    return jnp.moveaxis(parts, 0, dim).reshape(lengths)


def sent_to_all(value, axis):
    length = lax.axis_size(axis)
    return lax.all_to_all(
        jnp.broadcast_to(value[None], (length, *value.shape)), axis, 0, 0, tiled=True
    )


def gather_directly(value, axis, dim):
    return in_order(sent_to_all(value, axis), dim)


def in_one_piece(arrays, axis, dim, along):
    both = jnp.concatenate(arrays, axis=along)
    result, at, gathered = (lax.all_gather(both, axis, axis=dim, tiled=True), 0, [])
    for a in arrays:
        gathered.append(lax.slice_in_dim(result, at, at + a.shape[along], axis=along))
        at += a.shape[along]
    return tuple(gathered)


def split_up(value, dim, length):
    before, after = (value.shape[:dim], value.shape[dim + 1 :])
    return jnp.moveaxis(value.reshape(*before, length, -1, *after), dim, 0)


def sent_and_summed(value, axis, dim):
    length = lax.axis_size(axis)
    parts = lax.all_to_all(split_up(value, dim, length), axis, 0, 0, tiled=True)
    return jnp.sum(parts.astype(jnp.float32), axis=0)


def causal_taps(current, previous, kernel):
    tap_count = kernel.shape[0]
    length = current.shape[0]
    padded = jnp.concatenate([previous, current], 0).astype(jnp.float32)
    result = jnp.zeros((length, current.shape[1]), jnp.float32)
    for offset in range(tap_count):
        result = result + kernel[offset].astype(jnp.float32) * padded[offset : offset + length]
    return result


def channel_norm(stream, gain):
    floats = stream.astype(jnp.float32)
    scaled = floats * lax.rsqrt(jnp.mean(floats * floats, axis=-1, keepdims=True) + epsilon)
    return (scaled * gain).astype(jnp.bfloat16)


def on_device(
    mixer_value_projection,
    write_vectors_projected,
    read_vectors_projected,
    output_gate_projected,
    step_size_scores,
    position_decay_extra,
    step_size_bias,
    head_decay_logarithm,
    value_filter_taps,
    write_filter_taps,
    read_filter_taps,
    gated_group_norm_gain,
    mixer_output_weight,
    residual,
    feedforward_norm_gain,
    feedforward_gate_weight,
    feedforward_value_weight,
    gate_filter_taps,
    single_value_filter_taps,
    feedforward_down_weight,
):
    row_count = mixer_value_projection.shape[0]
    head_count = step_size_scores.shape[1]
    group_count = write_vectors_projected.shape[1] // STATE
    per_group = head_count // group_count
    mix_rim = value_filter_taps.shape[0] - 1
    rim_values, rim_write, rim_read = from_behind(
        (
            mixer_value_projection[row_count - mix_rim :],
            write_vectors_projected[row_count - mix_rim :],
            read_vectors_projected[row_count - mix_rim :],
        ),
        SP,
        1,
    )
    x_conv = jax.nn.silu(causal_taps(mixer_value_projection, rim_values, value_filter_taps)).astype(
        jnp.bfloat16
    )
    write_conv = jax.nn.silu(
        causal_taps(write_vectors_projected, rim_write, write_filter_taps)
    ).astype(jnp.bfloat16)
    read_conv = jax.nn.silu(causal_taps(read_vectors_projected, rim_read, read_filter_taps)).astype(
        jnp.bfloat16
    )
    step_size_head = jax.nn.softplus(step_size_scores + step_size_bias)
    logarithm_decay_rate = -step_size_head * jnp.exp(head_decay_logarithm) + position_decay_extra
    scaled = (
        x_conv.astype(jnp.float32).reshape(row_count, head_count, HEAD) * step_size_head[:, :, None]
    ).astype(jnp.bfloat16)
    block_count = row_count // BLOCK
    value_blocks = scaled.reshape(block_count, BLOCK, group_count, per_group, HEAD)
    write_blocks = write_conv.reshape(block_count, BLOCK, group_count, STATE)
    read_blocks = read_conv.reshape(block_count, BLOCK, group_count, STATE)
    running = jnp.cumsum(logarithm_decay_rate.reshape(block_count, BLOCK, head_count), axis=1)
    by_head = jnp.moveaxis(running, 1, 2)
    spread = by_head[..., :, None] - by_head[..., None, :]
    causal = jnp.tril(jnp.ones((BLOCK, BLOCK), dtype=jnp.bool_))
    decays = jnp.exp(jnp.where(causal, spread, -jnp.inf)).reshape(
        block_count, group_count, per_group, BLOCK, BLOCK
    )
    scores = jnp.einsum(
        "blgn,bsgn->bgls", read_blocks, write_blocks, preferred_element_type=jnp.float32
    )
    weights = (scores[:, :, None] * decays).astype(jnp.bfloat16)
    inside = jnp.einsum(
        "bgrls,bsgrp->blgrp", weights, value_blocks, preferred_element_type=jnp.float32
    )
    tails = jnp.moveaxis(jnp.exp(by_head[..., -1:] - by_head), 2, 1).reshape(
        block_count, BLOCK, group_count, per_group
    )
    tailed = (value_blocks.astype(jnp.float32) * tails[..., None]).astype(jnp.bfloat16)
    fresh = jnp.einsum(
        "bsgn,bsgrp->bgrnp", write_blocks, tailed, preferred_element_type=jnp.float32
    )
    block_logs = by_head[..., -1].reshape(block_count, group_count, per_group)

    def carry_step(carried, inputs):
        piece, block_log = inputs
        return (carried * jnp.exp(block_log)[..., None, None] + piece, carried)

    empty_state = jnp.zeros((group_count, per_group, STATE, HEAD), jnp.float32)
    local_end, local_before = lax.scan(carry_step, empty_state, (fresh, block_logs))
    device_log = jnp.sum(block_logs, axis=0)

    def combine(earlier, later):
        return (earlier[0] * later[0], earlier[1] * later[0][..., None, None] + later[1])

    identity = (jnp.ones((group_count, per_group), jnp.float32), empty_state)
    incoming = entering_2((jnp.exp(device_log), local_end), SP, combine, identity)[1]
    before_block = jnp.cumsum(block_logs, axis=0) - block_logs
    entering_state = local_before + incoming[None] * jnp.exp(before_block)[..., None, None]
    entering = jnp.einsum(
        "blgn,bgrnp->blgrp",
        read_blocks.astype(jnp.float32),
        entering_state,
        precision=lax.Precision.HIGHEST,
    )
    entering = (
        entering * jnp.exp(running).reshape(block_count, BLOCK, group_count, per_group)[..., None]
    )
    mixer = (inside + entering).reshape(row_count, head_count * HEAD)
    gated = (mixer * jax.nn.silu(output_gate_projected.astype(jnp.float32))).reshape(
        row_count, group_count, -1
    )
    gated = gated * lax.rsqrt(jnp.mean(gated * gated, axis=-1, keepdims=True) + epsilon)
    normed = (gated.reshape(row_count, -1) * gated_group_norm_gain).astype(jnp.bfloat16)
    share = row_count // lax.axis_size("tp")
    tp_index = lax.axis_index("tp")
    summed = lax.psum_scatter(
        jnp.dot(normed, mixer_output_weight, preferred_element_type=jnp.float32),
        "tp",
        scatter_dimension=0,
        tiled=True,
    )
    own_residual = lax.dynamic_slice_in_dim(residual, tp_index * share, share, 0)
    stream = (own_residual.astype(jnp.float32) + summed).astype(jnp.bfloat16)
    ffn_rows = gather_directly(channel_norm(stream, feedforward_norm_gain), "tp", 0)
    pieces = in_one_piece((feedforward_gate_weight, feedforward_value_weight), SP, 0, 1)
    gate_sum = jnp.dot(ffn_rows, pieces[0], preferred_element_type=jnp.float32)
    value_sum = jnp.dot(ffn_rows, pieces[1], preferred_element_type=jnp.float32)
    gate_rows = gate_sum.astype(jnp.bfloat16)
    value_rows = value_sum.astype(jnp.bfloat16)
    ffn_rim = gate_filter_taps.shape[0] - 1
    rim_gate, rim_value = from_behind(
        (gate_rows[row_count - ffn_rim :], value_rows[row_count - ffn_rim :]), SP, 1
    )
    hidden = (
        jax.nn.silu(causal_taps(gate_rows, rim_gate, gate_filter_taps))
        * causal_taps(value_rows, rim_value, single_value_filter_taps)
    ).astype(jnp.bfloat16)
    partial_down = jnp.dot(
        hidden,
        lax.all_gather(feedforward_down_weight, SP, axis=1, tiled=True),
        preferred_element_type=jnp.float32,
    )
    down = sent_and_summed(partial_down.astype(jnp.bfloat16), "tp", 0)
    return (stream.astype(jnp.float32) + down).astype(jnp.bfloat16)


def solution(mesh):
    torus = Mesh(mesh.devices.reshape(4, 4, 2, mesh.shape["tp"]), ("sp_0", "sp_1", "sp_2", "tp"))
    in_specs = (
        P(SP, "tp"),
        P(SP, "tp"),
        P(SP, "tp"),
        P(SP, "tp"),
        P(SP, "tp"),
        P(SP, "tp"),
        P("tp"),
        P("tp"),
        P(None, "tp"),
        P(None, "tp"),
        P(None, "tp"),
        P("tp"),
        P("tp", None),
        P(SP, None),
        P(),
        P(SP, "tp"),
        P(SP, "tp"),
        P(None, "tp"),
        P(None, "tp"),
        P("tp", SP),
    )
    out_specs = P(SP_TP, None)
    return jax.shard_map(
        on_device, mesh=torus, in_specs=in_specs, out_specs=out_specs, check_vma=False
    )
```

profile of v0, /device:TPU:1, one launch (start us, length us, event | category | flops | bytes accessed | tf_op | source)
XLA Modules:
  0.0 345.3 jit_solution(731696417473603664)
XLA Ops:
  9.0 4.6 %collective-permute-start = (bf16[3,512]{0,1:T(8,128)(2,1)}, bf16[3,512]{0,1:T(8,128)(2,1)}, u32[]{:S(2)}, u32[]{:S(2)}) collective-permute-start(bf16[3,512]{0,1:T(8,128)(2,1)} %copy.47), channel_id=1, source_target_pairs={{0,4},{4,8},{8,12},{12,16},{16,20},{20,24},{24,28},{28,32},{32,36}... | collective-permute-start | bytes 9224 | tf_op jit(solution)/shard_map/ppermute | solution.py:20
  15.0 1.9 collective-permute-start.2
  18.3 3.6 %collective-permute-start.1 = (bf16[3,64]{0,1:T(8,128)(2,1)}, bf16[3,64]{0,1:T(8,128)(2,1)}, u32[]{:S(2)}, u32[]{:S(2)}) collective-permute-start(bf16[3,64]{0,1:T(8,128)(2,1)} %slice.203), channel_id=1, source_target_pairs={{0,4},{4,8},{8,12},{12,16},{16,20},{20,24},{24,28},{28,32},{32,36}... | collective-permute-start | bytes 1160 | tf_op jit(solution)/shard_map/ppermute | solution.py:20
  34.0 2.5 all-reduce
  38.6 8.7 %all-reduce.1 = f32[32]{0:T(128)S(1)} all-reduce(f32[32]{0:T(128)S(1)} %fusion.73), channel_id=4, replica_groups=mesh['sp_0'=4,'sp_1'=4,'sp_2'=2,'tp'=4] {'sp_1'}, use_global_device_ids=true, to_apply=%add.1 | all-reduce | flops 32 | bytes 256
  50.1 7.2 %all_gather.34 = f32[4,1,8]{2,1,0:T(1,128)S(1)} all-gather(f32[1,1,8]{2,1,0:T(1,128)S(1)} %get-tuple-element.113), channel_id=1, replica_groups=mesh['sp_0'=4,'sp_1'=4,'sp_2'=2,'tp'=4] {'sp_0'}, dimensions={0}, use_global_device_ids=true | all-gather | bytes 160 | tf_op jit(solution)/shard_map/all_gather | solution.py:34
  60.7 1.7 copy.62
  62.4 2.3 copy.64
  66.6 1.6 fusion.61
  70.8 3.4 fusion.48
  74.1 2.7 reshape.357
  76.8 2.9 multiply_convert_fusion.1
  79.7 1.5 convolution_bitcast_fusion
  81.2 15.6 %while.13 = (s32[]{:T(128)}, f32[1,8,64,64]{3,2,1,0:T(8,128)S(1)}, f32[6,1,8,64,64]{4,3,2,1,0:T(8,128)}, f32[6,1,8]{2,1,0:T(1,128)}, f32[6,1,8,64,64]{3,4,2,0,1:T(8,128)}, /*index=5*/s32[]{:T(128)}, s32[]{:T(128)}) while((s32[]{:T(128)}, f32[1,8,64,64]{3,2,1,0:T(8,128)S(1)}, f32[6,1,8,64,64]{4,3,2,1,0:T(8,128)}, ...), condition=%wide.region_2.3_spmd.clone, body=%wide.region_1.2_spmd.clone.sunk | while | flops 131075 | bytes 1311424 | solution.py:179
  96.9 6.0 %all-gather.1 = f32[2,8,64,64]{3,2,1,0:T(8,128)S(1)} all-gather(f32[1,8,64,64]{3,2,1,0:T(8,128)S(1)} %get-tuple-element.34), channel_id=3, replica_groups=mesh['sp_0'=4,'sp_1'=4,'sp_2'=2,'tp'=4] {'sp_2'}, dimensions={0}, use_global_device_ids=true | all-gather | bytes 393216 | tf_op jit(solution)/shard_map/all_gather | solution.py:34
  103.1 12.3 %all_gather.37 = f32[4,1,8,64,64]{4,3,2,1,0:T(8,128)S(1)} all-gather(f32[1,1,8,64,64]{4,3,2,1,0:T(8,128)S(1)} %fusion.53), channel_id=1, replica_groups=mesh['sp_0'=4,'sp_1'=4,'sp_2'=2,'tp'=4] {'sp_1'}, dimensions={0}, use_global_device_ids=true | all-gather | bytes 655360 | tf_op jit(solution)/shard_map/all_gather | solution.py:34
  115.6 13.0 %all_gather.38 = f32[4,1,8,64,64]{4,3,2,1,0:T(8,128)S(1)} all-gather(f32[1,1,8,64,64]{4,3,2,1,0:T(8,128)S(1)} %slice_add_fusion.4), channel_id=1, replica_groups=mesh['sp_0'=4,'sp_1'=4,'sp_2'=2,'tp'=4] {'sp_0'}, dimensions={0}, use_global_device_ids=true | all-gather | bytes 655360 | tf_op jit(solution)/shard_map/all_gather | solution.py:34
  129.1 1.5 fusion.32
  133.6 4.8 %fusion.41 = f32[768,2048]{1,0:T(8,128)} fusion(bf16[512,2048]{1,0:T(8,128)(2,1)S(1)} %copy-done, f32[512]{0:T(512)S(1)} %copy-done.33, f32[768]{0:T(1024)S(1)} %add_rsqrt_fusion, bf16[768,512]{0,1:T(8,128)(2,1)S(1)} %copy-done.2, f32[64,8,6,128]{3,2,1,0:T(8,128)S(1)} %bitcast.139), kind=kOutput, calls=%fused_computation.69 | convolution fusion | flops 1614151680 | bytes 10753024 | tf_op jit(solution)/shard_map/dot_general | solution.py:207
  140.8 64.3 %reduce-scatter.2.cloned.1.call-done = f32[192,2048]{1,0:T(8,128)} async-done(((f32[768,2048]{1,0:T(8,128)}), f32[192,2048]{1,0:T(8,128)}) %reduce-scatter.2.cloned.1.call-update) | async-done | bytes 1572880 | tf_op jit(solution)/shard_map/reduce_scatter | solution.py:206
  205.1 1.9 fusion.23
  207.3 2.0 broadcast_in_dim.34
  209.3 4.8 %all-to-all-start = ((bf16[4,192,2048]{2,1,0:T(8,128)(2,1)}), bf16[4,192,2048]{2,1,0:T(8,128)(2,1)}, u32[]{:S(2)}, u32[]{:S(2)}) async-start(bf16[4,192,2048]{2,1,0:T(8,128)(2,1)} %broadcast_in_dim.34), calls=%async_computation.1 | async-start | bytes 6291456 | tf_op jit(solution)/shard_map/all_to_all | solution.py:52
  214.3 36.9 %all-to-all-done = bf16[4,192,2048]{2,1,0:T(8,128)(2,1)} async-done(((bf16[4,192,2048]{2,1,0:T(8,128)(2,1)}), bf16[4,192,2048]{2,1,0:T(8,128)(2,1)}, u32[]{:S(2)}, u32[]{:S(2)}) %all-to-all-start) | async-done | bytes 3145760 | tf_op jit(solution)/shard_map/all_to_all | solution.py:52
  251.1 8.5 %fusion.12 = bf16[768,1408]{1,0:T(8,128)(2,1)S(1)} fusion(bf16[768,2048]{1,0:T(8,128)(2,1)} %bitcast.35, bf16[2048,2816]{1,0:T(8,128)(2,1)} %all-gather.6.cloned.1.call-done), kind=kOutput, calls=%fused_computation.23 | convolution fusion | flops 4430266368 | bytes 11075584 | tf_op jit(solution)/shard_map/dot_general | solution.py:216
  259.7 4.6 %collective-permute-start.3 = (bf16[2,1408]{1,0:T(2,128)(2,1)S(1)}, bf16[2,1408]{1,0:T(2,128)(2,1)S(1)}, u32[]{:S(2)}, u32[]{:S(2)}) collective-permute-start(bf16[2,1408]{1,0:T(2,128)(2,1)S(1)} %slice.293), channel_id=1, source_target_pairs={{0,4},{4,8},{8,12},{12,16},{16,20},{20,24},{24,28},{28,32},{32,36}... | collective-permute-start | bytes 16904 | tf_op jit(solution)/shard_map/ppermute | solution.py:20
  264.2 6.7 %fusion.15 = bf16[768,1408]{1,0:T(8,128)(2,1)S(1)} fusion(bf16[768,2048]{1,0:T(8,128)(2,1)} %bitcast.35, bf16[2048,2816]{1,0:T(8,128)(2,1)S(1)} %copy-done.32), kind=kOutput, calls=%fused_computation.24 | convolution fusion | flops 4430266368 | bytes 11075584 | tf_op jit(solution)/shard_map/dot_general | solution.py:217
  271.0 2.1 collective-permute-start.4
  273.1 2.5 maximum_convert_fusion
  275.6 2.4 maximum_convert_fusion.1
  278.1 17.3 %convolution_convert_fusion = bf16[768,2048]{1,0:T(8,128)(2,1)} fusion(bf16[1408,2048]{0,1:T(8,128)(2,1)} %all-gather.8.cloned.1.call-done, f32[770,1408]{1,0:T(8,128)} %maximum_convert_fusion.1, f32[770,1408]{1,0:T(8,128)} %maximum_convert_fusion, f32[1408]{0:T(1024)S(1)} %get-tuple-element.72, f32[1408]{0:T(1024)S(1)} %get-tuple-element.73, ...), kind=kOutput, calls=%fused_computation.25 | convolution fusion | flops 4448059392 | bytes 34898944 | tf_op jit(solution)/shard_map/dot_general | solution.py:228
  295.4 40.8 %all_to_all.10 = bf16[4,192,2048]{2,1,0:T(8,128)(2,1)S(1)} all-to-all(bf16[4,192,2048]{2,1,0:T(8,128)(2,1)} %bitcast.142), channel_id=1, replica_groups=mesh['sp_0'=4,'sp_1'=4,'sp_2'=2,'tp'=4] {'tp'}, dimensions={0} | all-to-all | bytes 6291456 | tf_op jit(solution)/shard_map/all_to_all | solution.py:77
  (167 shorter events, 51.4 us)
Async XLA Ops:
  7.4 126.2 %copy-start = (bf16[512,2048]{1,0:T(8,128)(2,1)S(1)}, bf16[512,2048]{1,0:T(8,128)(2,1)}, u32[]{:S(2)}) copy-start(bf16[512,2048]{1,0:T(8,128)(2,1)} %param.34) | copy-start | bytes 6291460
  7.4 197.7 %reduce-scatter.2.cloned.1.call-start = ((), (), s32[]{:S(2)}) async-start(), calls=%async_computation.3 | async-start | bytes 7864320 | tf_op jit(solution)/shard_map/reduce_scatter | solution.py:206
  9.0 60.4 %collective-permute-start = (bf16[3,512]{0,1:T(8,128)(2,1)}, bf16[3,512]{0,1:T(8,128)(2,1)}, u32[]{:S(2)}, u32[]{:S(2)}) collective-permute-start(bf16[3,512]{0,1:T(8,128)(2,1)} %copy.47), channel_id=1, source_target_pairs={{0,4},{4,8},{8,12},{12,16},{16,20},{20,24},{24,28},{28,32},{32,36}... | collective-permute-start | bytes 9224 | tf_op jit(solution)/shard_map/ppermute | solution.py:20
  15.0 49.7 %collective-permute-start.2 = (bf16[3,64]{0,1:T(8,128)(2,1)}, bf16[3,64]{0,1:T(8,128)(2,1)}, u32[]{:S(2)}, u32[]{:S(2)}) collective-permute-start(bf16[3,64]{0,1:T(8,128)(2,1)} %slice.212), channel_id=1, source_target_pairs={{0,4},{4,8},{8,12},{12,16},{16,20},{20,24},{24,28},{28,32},{32,36}... | collective-permute-start | bytes 1160 | tf_op jit(solution)/shard_map/ppermute | solution.py:20
  18.3 47.5 %collective-permute-start.1 = (bf16[3,64]{0,1:T(8,128)(2,1)}, bf16[3,64]{0,1:T(8,128)(2,1)}, u32[]{:S(2)}, u32[]{:S(2)}) collective-permute-start(bf16[3,64]{0,1:T(8,128)(2,1)} %slice.203), channel_id=1, source_target_pairs={{0,4},{4,8},{8,12},{12,16},{16,20},{20,24},{24,28},{28,32},{32,36}... | collective-permute-start | bytes 1160 | tf_op jit(solution)/shard_map/ppermute | solution.py:20
  21.9 25.4 %copy-start.15 = (bf16[4,512]{1,0:T(4,128)(2,1)S(1)}, bf16[4,512]{1,0:T(4,128)(2,1)}, u32[]{:S(2)}) copy-start(bf16[4,512]{1,0:T(4,128)(2,1)} %param.30) | copy-start | bytes 12292
  30.7 33.9 %copy-start.8 = (bf16[768,64]{0,1:T(8,128)(2,1)S(1)}, bf16[768,64]{0,1:T(8,128)(2,1)}, u32[]{:S(2)}) copy-start(bf16[768,64]{0,1:T(8,128)(2,1)} %param.23) | copy-start | bytes 294916
  30.7 35.0 %copy-start.9 = (bf16[768,64]{0,1:T(8,128)(2,1)S(1)}, bf16[768,64]{0,1:T(8,128)(2,1)}, u32[]{:S(2)}) copy-start(bf16[768,64]{0,1:T(8,128)(2,1)} %param.24) | copy-start | bytes 294916
  68.2 2.6 copy-start.19
  81.2 21.7 %copy-start.24 = (f32[8]{0:T(128)S(1)}, f32[8]{0:T(128)}, u32[]{:S(2)}) copy-start(f32[8]{0:T(128)} %get-tuple-element.114) | copy-start | bytes 100
  81.2 21.7 %copy-start.25 = (f32[8]{0:T(128)S(1)}, f32[8]{0:T(128)}, u32[]{:S(2)}) copy-start(f32[8]{0:T(128)} %get-tuple-element.115) | copy-start | bytes 100
  96.8 18.6 %copy-start.20 = (f32[8]{0:T(128)S(1)}, f32[8]{0:T(128)}, u32[]{:S(2)}) copy-start(f32[8]{0:T(128)} %get-tuple-element.116) | copy-start | bytes 100
  96.9 18.5 %copy-start.21 = (f32[8]{0:T(128)S(1)}, f32[8]{0:T(128)}, u32[]{:S(2)}) copy-start(f32[8]{0:T(128)} %get-tuple-element.117) | copy-start | bytes 100
  96.9 18.5 %copy-start.22 = (f32[8]{0:T(128)S(1)}, f32[8]{0:T(128)}, u32[]{:S(2)}) copy-start(f32[8]{0:T(128)} %get-tuple-element.118) | copy-start | bytes 100
  96.9 18.5 %copy-start.23 = (f32[8]{0:T(128)S(1)}, f32[8]{0:T(128)}, u32[]{:S(2)}) copy-start(f32[8]{0:T(128)} %get-tuple-element.119) | copy-start | bytes 100
  103.0 25.5 %copy-start.26 = (f32[8]{0:T(128)S(1)}, f32[8]{0:T(128)}, u32[]{:S(2)}) copy-start(f32[8]{0:T(128)} %get-tuple-element.86) | copy-start | bytes 100
  103.0 25.5 %copy-start.27 = (f32[8]{0:T(128)S(1)}, f32[8]{0:T(128)}, u32[]{:S(2)}) copy-start(f32[8]{0:T(128)} %get-tuple-element.87) | copy-start | bytes 100
  103.0 25.5 %copy-start.28 = (f32[8]{0:T(128)S(1)}, f32[8]{0:T(128)}, u32[]{:S(2)}) copy-start(f32[8]{0:T(128)} %get-tuple-element.101) | copy-start | bytes 100
  103.0 25.5 %copy-start.29 = (f32[8]{0:T(128)S(1)}, f32[8]{0:T(128)}, u32[]{:S(2)}) copy-start(f32[8]{0:T(128)} %get-tuple-element.102) | copy-start | bytes 100
  103.0 25.5 %copy-start.30 = (f32[8]{0:T(128)S(1)}, f32[8]{0:T(128)}, u32[]{:S(2)}) copy-start(f32[8]{0:T(128)} %get-tuple-element.103) | copy-start | bytes 100
  103.1 25.5 %copy-start.31 = (f32[8]{0:T(128)S(1)}, f32[8]{0:T(128)}, u32[]{:S(2)}) copy-start(f32[8]{0:T(128)} %get-tuple-element.104) | copy-start | bytes 100
  115.6 13.5 %copy-start.3 = (f32[6,1,8,64,64]{4,3,2,1,0:T(8,128)S(1)}, f32[6,1,8,64,64]{4,3,2,1,0:T(8,128)}, u32[]{:S(2)}) copy-start(f32[6,1,8,64,64]{4,3,2,1,0:T(8,128)} %get-tuple-element.33) | copy-start | bytes 2359300
  115.6 13.5 %copy-start.5 = (bf16[6,128,64]{1,0,2:T(8,128)(2,1)S(1)}, bf16[6,128,64]{1,0,2:T(8,128)(2,1)}, u32[]{:S(2)}) copy-start(bf16[6,128,64]{1,0,2:T(8,128)(2,1)} %reshape.345) | copy-start | bytes 294916
  138.4 68.6 %copy-start.16 = (f32[2048]{0:T(1024)S(1)}, f32[2048]{0:T(1024)}, u32[]{:S(2)}) copy-start(f32[2048]{0:T(1024)} %param.36) | copy-start | bytes 24580
  138.4 112.7 %all-gather.6.cloned.1.call-start = ((), (), s32[]{:S(2)}) async-start(), calls=%async_computation.4 | async-start | bytes 11894784 | tf_op jit(solution)/shard_map/all_gather | solution.py:63
  140.2 137.9 %all-gather.8.cloned.1.call-start = ((), (), s32[]{:S(2)}) async-start(), calls=%async_computation.5 | async-start | bytes 5947392 | tf_op jit(solution)/shard_map/all_gather | solution.py:230
  209.3 4.8 %copy-start.10 = (bf16[3,1408]{1,0:T(4,128)(2,1)S(1)}, bf16[3,1408]{1,0:T(4,128)(2,1)}, u32[]{:S(2)}) copy-start(bf16[3,1408]{1,0:T(4,128)(2,1)} %param.40) | copy-start | bytes 25348
  209.3 4.8 %copy-start.11 = (bf16[3,1408]{1,0:T(4,128)(2,1)S(1)}, bf16[3,1408]{1,0:T(4,128)(2,1)}, u32[]{:S(2)}) copy-start(bf16[3,1408]{1,0:T(4,128)(2,1)} %param.39) | copy-start | bytes 25348
  209.3 41.8 %all-to-all-start = ((bf16[4,192,2048]{2,1,0:T(8,128)(2,1)}), bf16[4,192,2048]{2,1,0:T(8,128)(2,1)}, u32[]{:S(2)}, u32[]{:S(2)}) async-start(bf16[4,192,2048]{2,1,0:T(8,128)(2,1)} %broadcast_in_dim.34), calls=%async_computation.1 | async-start | bytes 6291456 | tf_op jit(solution)/shard_map/all_to_all | solution.py:52
  251.1 13.1 %copy-start.32 = (bf16[2048,2816]{1,0:T(8,128)(2,1)S(1)}, bf16[2048,2816]{1,0:T(8,128)(2,1)}, u32[]{:S(2)}) copy-start(bf16[2048,2816]{1,0:T(8,128)(2,1)} %all-gather.6.cloned.1.call-done) | copy-start | bytes 34603012
  259.7 13.4 %collective-permute-start.3 = (bf16[2,1408]{1,0:T(2,128)(2,1)S(1)}, bf16[2,1408]{1,0:T(2,128)(2,1)S(1)}, u32[]{:S(2)}, u32[]{:S(2)}) collective-permute-start(bf16[2,1408]{1,0:T(2,128)(2,1)S(1)} %slice.293), channel_id=1, source_target_pairs={{0,4},{4,8},{8,12},{12,16},{16,20},{20,24},{24,28},{28,32},{32,36}... | collective-permute-start | bytes 16904 | tf_op jit(solution)/shard_map/ppermute | solution.py:20
  271.0 4.7 %collective-permute-start.4 = (bf16[2,1408]{1,0:T(2,128)(2,1)S(1)}, bf16[2,1408]{1,0:T(2,128)(2,1)S(1)}, u32[]{:S(2)}, u32[]{:S(2)}) collective-permute-start(bf16[2,1408]{1,0:T(2,128)(2,1)S(1)} %slice.298), channel_id=1, source_target_pairs={{0,4},{4,8},{8,12},{12,16},{16,20},{20,24},{24,28},{28,32},{32,36}... | collective-permute-start | bytes 16904 | tf_op jit(solution)/shard_map/ppermute | solution.py:20
  (12 other events, 18.4 us)
Sparse Core Ops, SparseCore 0:
  138.5 66.5 reduce-scatter.1
Sparse Core Ops, SparseCore 1:
  141.2 63.3 all-gather.5
  206.6 47.6 all-gather.7
where the time goes:
time: 347 us; the launch traced here: 345 us
  waiting for transfers between devices  102 us (29%)
  blocking collectives  90.5 us (26%)
  matrix products  43.1 us (12%)
  local copies, waits for them, and re-layouts  36.4 us (10%)
  other arithmetic  34.8 us (10%)
  starting transfers between devices  21.6 us (6%)
  between operations  16.8 us (5%)
    reduce_scatter x1, waiting for transfers between devices, on_device(): lax.psum_scatter(jnp.dot(normed, mixer_output_weight, preferred_element_t...  64.3 us
    all_to_all x1, blocking collectives, sent_and_summed(): parts = lax.all_to_all(split_up(value, dim, length), axis, 0, 0, tiled=True)  40.8 us
    all_gather x4, blocking collectives, entering_2(): pieces = jax.tree.map(lambda part: lax.all_gather(part, axis), running)  38.5 us
    all_to_all x1, waiting for transfers between devices, sent_to_all(): lax.all_to_all(jnp.broadcast_to(value[None], (length, *value.shape)), axi...  36.9 us
    dot_general x1, matrix products, on_device(): jnp.dot(hidden, lax.all_gather(feedforward_down_weight, SP, axis=1, tiled...  17.3 us
    ppermute x5, starting transfers between devices, from_behind(): return lax.ppermute(value, axis, pairs)  16.8 us
    unnamed x2, blocking collectives  11.2 us
    dot_general x1, matrix products, on_device(): gate_sum = jnp.dot(ffn_rows, pieces[0], preferred_element_type=jnp.float32)  8.51 us
  transfers between devices with their start and end apart: 9, of which 2 were waited for; matrix products, arithmetic and copies ran while one was open for 16% of the time, Pallas kernels for 0%

commit v1 on v0

v1 whole, which is shorter than its diff:
```python
import jax
import jax.numpy as jnp
from jax import lax
from jax.experimental import pallas as pl
from jax.experimental.pallas import tpu as pltpu
from jax.sharding import Mesh
from jax.sharding import PartitionSpec as P


HEAD = 64
STATE = 64
BLOCK = 128
RIM = 16
SP = ("sp_0", "sp_1", "sp_2")
SP_TP = ("sp_0", "sp_1", "sp_2", "tp")
BF = jnp.bfloat16
F32 = jnp.float32
HIGH = lax.Precision.HIGHEST

epsilon = 1e-06


def shifted(value, axis, by, wrap=False):
    length = lax.axis_size(axis)
    if wrap:
        pairs = [(i, (i + by) % length) for i in range(length)]
    else:
        pairs = [(i, i + by) for i in range(length) if 0 <= i + by < length]
    return lax.ppermute(value, axis, pairs)


def swapped(value):
    return lax.ppermute(value, "sp_2", [(0, 1), (1, 0)])


def turned(value, phase, by):
    zs, ys, cs = (lax.axis_size(axis) for axis in SP)
    pairs = []
    for z in range(zs):
        for y in range(ys):
            for c in range(cs):
                to_z, to_y = (z, (y + by) % ys) if c == phase else ((z + by) % zs, y)
                pairs.append(((z * ys + y) * cs + c, (to_z * ys + to_y) * cs + c))
    return lax.ppermute(value, SP, pairs)


def ring_of(step, value):
    half = value.shape[0] // 2
    behind = step(value, 1)
    ahead = step(value, -1)
    far_behind = step(behind[:half], 1)
    far_ahead = step(ahead[half:], -1)
    return behind, ahead, far_behind, far_ahead


def turned_ring(value, phase):
    return ring_of(lambda a, by: turned(a, phase, by), value)


def named_swaps(values):
    result = []
    for value in values:
        result.append(swapped(value))
    return result


def sent_to_all(value, axis):
    length = lax.axis_size(axis)
    return lax.all_to_all(
        jnp.broadcast_to(value[None], (length, *value.shape)), axis, 0, 0, tiled=True
    )


def silu(v):
    return v / (1.0 + jnp.exp(-v))


def rolled_taps(before, current, taps):
    count = taps.shape[0]
    rows = current.shape[0]
    padded = jnp.concatenate([before, current], 0)
    result = taps[count - 1 : count].astype(F32) * current
    for back in range(1, count):
        moved = pltpu.roll(padded, back, 0)[8 : 8 + rows]
        result = result + taps[count - 1 - back : count - back].astype(F32) * moved
    return result


def mixer_kernel(
    x_ref, w_ref, r_ref, hx_ref, hw_ref, hr_ref, dt_ref, ex_ref, bias_ref, rate_ref,
    tx_ref, tw_ref, tr_ref,
    y_ref, read_ref, grow_ref, state_ref,
    carry, total, bx, bw, br,
):
    step_index = pl.program_id(0)
    heads = dt_ref.shape[1]
    inner = x_ref.shape[1]

    @pl.when(step_index == 0)
    def _():
        carry[...] = jnp.zeros_like(carry)
        total[...] = jnp.zeros_like(total)
        bx[...] = hx_ref[RIM - 8 :, :].astype(F32)
        bw[...] = hw_ref[RIM - 8 :, :].astype(F32)
        br[...] = hr_ref[RIM - 8 :, :].astype(F32)

    cx = x_ref[...].astype(F32)
    cw = w_ref[...].astype(F32)
    cr = r_ref[...].astype(F32)
    x = silu(rolled_taps(bx[...], cx, tx_ref[...])).astype(BF)
    write = silu(rolled_taps(bw[...], cw, tw_ref[...])).astype(BF)
    read = silu(rolled_taps(br[...], cr, tr_ref[...])).astype(BF)
    bx[...] = cx[BLOCK - 8 :]
    bw[...] = cw[BLOCK - 8 :]
    br[...] = cr[BLOCK - 8 :]

    spread_of = (
        lax.broadcasted_iota(jnp.int32, (heads, inner), 1) // HEAD
        == lax.broadcasted_iota(jnp.int32, (heads, inner), 0)
    ).astype(F32)

    def spread(a):
        return jnp.dot(a, spread_of, precision=HIGH, preferred_element_type=F32)

    raw = dt_ref[...] + bias_ref[...]
    step = jnp.maximum(raw, 0.0) + jnp.log1p(jnp.exp(-jnp.abs(raw)))
    log_decay = -step * jnp.exp(rate_ref[...]) + ex_ref[...]
    rows = lax.broadcasted_iota(jnp.int32, (BLOCK, BLOCK), 0)
    cols = lax.broadcasted_iota(jnp.int32, (BLOCK, BLOCK), 1)
    causal = rows >= cols
    lower = causal.astype(F32)
    cum = jnp.dot(lower, log_decay, precision=HIGH, preferred_element_type=F32)
    cum_t = lax.dot_general(
        log_decay, lower, (((0,), (1,)), ((), ())), precision=HIGH, preferred_element_type=F32
    )
    scaled = (x.astype(F32) * spread(step)).astype(BF)
    scores = lax.dot_general(
        read, write, (((1,), (1,)), ((), ())), preferred_element_type=F32
    )
    first_half = lax.broadcasted_iota(jnp.int32, (BLOCK, 2 * HEAD), 1) < HEAD
    pieces = []
    for pair in range(heads // 2):
        values = scaled[:, pair * 2 * HEAD : (pair + 1) * 2 * HEAD]
        both = []
        for h in (2 * pair, 2 * pair + 1):
            gap = cum[:, h : h + 1] - cum_t[h : h + 1, :]
            weights = (scores * jnp.exp(jnp.where(causal, gap, -1e30))).astype(BF)
            both.append(jnp.dot(weights, values, preferred_element_type=F32))
        pieces.append(jnp.where(first_half, both[0], both[1]))
    inside = jnp.concatenate(pieces, 1)
    grown = spread(jnp.exp(cum))
    entering = jnp.dot(read.astype(F32), carry[...], precision=HIGH, preferred_element_type=F32)
    y_ref[...] = inside + grown * entering
    read_ref[...] = read
    grow_ref[...] = jnp.exp(cum + total[...][:1])
    tails = jnp.exp(cum[BLOCK - 1 :] - cum)
    tailed = (scaled.astype(F32) * spread(tails)).astype(BF)
    fresh = lax.dot_general(
        write, tailed, (((0,), (0,)), ((), ())), preferred_element_type=F32
    )
    new_state = carry[...] * grown[BLOCK - 1 :] + fresh
    new_total = total[...] + cum[BLOCK - 1 :]
    carry[...] = new_state
    total[...] = new_total

    @pl.when(step_index == pl.num_programs(0) - 1)
    def _():
        state_ref[:STATE, :] = new_state.astype(BF)
        decay = spread(jnp.exp(new_total))
        state_ref[STATE:, :] = jnp.concatenate([decay, decay], 0).astype(BF)


def mixer_local(x, w, r, hx, hw, hr, dt, ex, bias, rate, tx, tw, tr):
    rows, inner = x.shape
    heads = dt.shape[1]
    by_block = lambda width: pl.BlockSpec((BLOCK, width), lambda b: (b, 0))
    whole = lambda a: pl.BlockSpec(a.shape, lambda b: (0, 0))
    return pl.pallas_call(
        mixer_kernel,
        grid=(rows // BLOCK,),
        in_specs=[by_block(inner), by_block(STATE), by_block(STATE)]
        + [whole(a) for a in (hx, hw, hr)]
        + [by_block(heads), by_block(heads)]
        + [whole(a) for a in (bias, rate, tx, tw, tr)],
        out_specs=[
            by_block(inner),
            by_block(STATE),
            by_block(heads),
            pl.BlockSpec((STATE + RIM, inner), lambda b: (0, 0)),
        ],
        out_shape=[
            jax.ShapeDtypeStruct((rows, inner), F32),
            jax.ShapeDtypeStruct((rows, STATE), BF),
            jax.ShapeDtypeStruct((rows, heads), F32),
            jax.ShapeDtypeStruct((STATE + RIM, inner), BF),
        ],
        scratch_shapes=[
            pltpu.VMEM((STATE, inner), F32),
            pltpu.VMEM((8, heads), F32),
            pltpu.VMEM((8, inner), F32),
            pltpu.VMEM((8, STATE), F32),
            pltpu.VMEM((8, STATE), F32),
        ],
        name="mixer_local",
    )(x, w, r, hx, hw, hr, dt, ex, bias, rate, tx, tw, tr)


def finish_kernel(y_ref, read_ref, grow_ref, gate_ref, state_ref, gain_ref, out_ref):
    heads = grow_ref.shape[1]
    inner = y_ref.shape[1]
    spread_of = (
        lax.broadcasted_iota(jnp.int32, (heads, inner), 1) // HEAD
        == lax.broadcasted_iota(jnp.int32, (heads, inner), 0)
    ).astype(F32)
    grown = jnp.dot(grow_ref[...], spread_of, precision=HIGH, preferred_element_type=F32)
    entering = jnp.dot(
        read_ref[...].astype(F32), state_ref[...], precision=HIGH, preferred_element_type=F32
    )
    mixer = y_ref[...] + grown * entering
    gated = mixer * silu(gate_ref[...].astype(F32))
    mean = jnp.mean(gated * gated, axis=-1, keepdims=True)
    out_ref[...] = (gated * lax.rsqrt(mean + epsilon) * gain_ref[...]).astype(BF)


def mixer_finish(y, read, grow, gate, state, gain):
    rows, inner = y.shape
    heads = grow.shape[1]
    size = 256
    by_block = lambda width: pl.BlockSpec((size, width), lambda b: (b, 0))
    whole = lambda a: pl.BlockSpec(a.shape, lambda b: (0, 0))
    return pl.pallas_call(
        finish_kernel,
        grid=(rows // size,),
        in_specs=[by_block(inner), by_block(STATE), by_block(heads), by_block(inner)]
        + [whole(state), whole(gain)],
        out_specs=by_block(inner),
        out_shape=jax.ShapeDtypeStruct((rows, inner), BF),
        name="mixer_finish",
    )(y, read, grow, gate, state, gain)


def split_state(packed):
    packed = packed.astype(F32)
    return packed[..., STATE : STATE + 1, :], packed[..., :STATE, :]


def joined(earlier, later):
    return earlier[0] * later[0], earlier[1] * later[0] + later[1]


def packed_state(pair):
    decay = jnp.broadcast_to(pair[0], (RIM, pair[0].shape[1]))
    return jnp.concatenate([pair[1], decay], 0).astype(BF)


def state_before(packed):
    own = split_state(packed)
    other = split_state(swapped(packed))
    late = lax.axis_index("sp_2") == 1
    first = jax.tree.map(lambda a, b: jnp.where(late, a, b), other, own)
    second = jax.tree.map(lambda a, b: jnp.where(late, a, b), own, other)
    running = joined(first, second)
    before = (
        jnp.where(late, other[0], 1.0),
        jnp.where(late, other[1], 0.0),
    )
    for axis in ("sp_1", "sp_0"):
        here = lax.axis_index(axis)
        all_of = sent_to_all(packed_state(running), axis)
        decay, state = split_state(all_of)
        whole = (jnp.ones_like(decay[0]), jnp.zeros_like(state[0]))
        inside = whole
        for k in range(lax.axis_size(axis)):
            whole = joined(whole, (decay[k], state[k]))
            passed = k < here
            inside = jax.tree.map(lambda new, old: jnp.where(passed, new, old), whole, inside)
        before = joined(inside, before)
        running = whole
    return before[1]


def gathered_ring(value, axis):
    return ring_of(lambda a, by: shifted(a, axis, by, True), value)


def summed_ring(here, on, back, far_on, far_back, axis):
    half = far_on.shape[0]
    more_on = shifted(far_on, axis, 1, True)
    more_back = shifted(far_back, axis, -1, True)
    on = jnp.concatenate(
        [(on[:half].astype(F32) + more_on.astype(F32)).astype(BF), on[half:]], 0
    )
    back = jnp.concatenate(
        [back[:half], (back[half:].astype(F32) + more_back.astype(F32)).astype(BF)], 0
    )
    from_behind = shifted(on, axis, 1, True)
    from_ahead = shifted(back, axis, -1, True)
    return here.astype(F32) + from_behind.astype(F32) + from_ahead.astype(F32)


def rolled(rows, taps):
    count = taps.shape[0]
    result = taps[count - 1 : count] * rows
    for back in range(1, count):
        result = result + taps[count - 1 - back : count - back] * pltpu.roll(rows, back, 0)
    return result


HOPS = (0, -1, 1, 2)


def ffn_kernel(
    place_ref, p0, p1, p2, p3a, p3b, halo, res_ref, hres_ref,
    o0, ob, oa, ofb, ofa, tb, ta, tfb, tfa,
    w0, wb, wa, wfb, wfa, s0, sb, sa, sfb, sfa,
    gain_ref, tg_ref, tv_ref,
    q0, q1, q3, q2a, q2b, own_ref,
    x, wo, wall, stream, xin, hid, part, sem_x, sem_o, sem_w, sem_q,
):
    z_index = place_ref[0]
    y_index = place_ref[1]
    core = place_ref[2]
    tp_index = place_ref[3]
    rows = res_ref.shape[0]
    width = res_ref.shape[1]
    inner = p0.shape[1]
    units = hid.shape[1]
    half = inner // 2
    copies_x, copies_o, copies_w = [], [], []

    def go(into, src, dst, sems):
        copy = pltpu.make_async_copy(src, dst, sems.at[len(into)])
        copy.start()
        into.append(copy)

    for k, by in enumerate(HOPS):
        at = lax.rem(tp_index + (by + 4), 4)
        columns = pl.ds(k * inner, inner)
        if k < 3:
            go(copies_x, (p0, p1, p2)[k], x.at[pl.ds(RIM, rows), columns], sem_x)
        else:
            go(copies_x, p3a, x.at[pl.ds(RIM, rows // 2), columns], sem_x)
            go(copies_x, p3b, x.at[pl.ds(RIM + rows // 2, rows // 2), columns], sem_x)
        go(copies_x, halo.at[at], x.at[pl.ds(0, RIM), columns], sem_x)
    go(copies_o, o0, wo.at[pl.ds(0, inner)], sem_o)
    for side, (b, a, fb, fa) in ((core, (ob, oa, ofb, ofa)), (1 - core, (tb, ta, tfb, tfa))):
        first = pl.multiple_of(side * half, half)
        go(copies_o, b, wo.at[pl.ds(inner + first, half)], sem_o)
        go(copies_o, a, wo.at[pl.ds(2 * inner + first, half)], sem_o)
        go(copies_o, fb, wo.at[pl.ds(3 * inner + first, half // 2)], sem_o)
        go(copies_o, fa, wo.at[pl.ds(3 * inner + first + half // 2, half // 2)], sem_o)
    for side, (o, b, a, fb, fa) in (
        (core, (w0, wb, wa, wfb, wfa)),
        (1 - core, (s0, sb, sa, sfb, sfa)),
    ):
        first_axis = jnp.where(side == 0, y_index, z_index)
        second_axis = jnp.where(side == 0, z_index, y_index)
        for m, by_second in enumerate(HOPS):
            second = lax.rem(second_axis + (by_second + 4), 4)
            for k, by_first in enumerate(HOPS):
                first = lax.rem(first_axis + (by_first + 4), 4)
                chip = jnp.where(side == 0, second * 4 + first, first * 4 + second)
                if m < 3:
                    src = (o, b, a)[m].at[k]
                else:
                    src = (fb, fa)[k // 2].at[k % 2]
                go(copies_w, src, wall.at[chip, :, side], sem_w)

    for copy in copies_x:
        copy.wait()
    for copy in copies_o:
        copy.wait()
    squares = jnp.zeros((rows + RIM, 1), F32)
    blocks = width // 512
    for n in range(blocks):
        columns = slice(n * 512, (n + 1) * 512)
        before = jnp.concatenate([hres_ref[:, columns], res_ref[:, columns]], 0).astype(F32)
        total = before + jnp.dot(x[...], wo[:, columns], preferred_element_type=F32)
        kept = total.astype(BF)
        stream[:, columns] = kept
        wide = kept.astype(F32)
        squares = squares + jnp.sum(wide * wide, axis=-1, keepdims=True)
    scale = lax.rsqrt(squares / width + epsilon)
    for n in range(blocks):
        columns = slice(n * 512, (n + 1) * 512)
        xin[:, columns] = (
            stream[:, columns].astype(F32) * scale * gain_ref[:, columns]
        ).astype(BF)
    share = rows // 4
    own_ref[...] = stream[pl.ds(pl.multiple_of(RIM + tp_index * share, 16), share), :]

    for copy in copies_w:
        copy.wait()
    for at in range(0, units, 384):
        size = min(384, units - at)
        columns = slice(at, at + size)
        gate_weight = wall[..., at : at + size].reshape(width, size)
        value_weight = wall[..., units + at : units + at + size].reshape(width, size)
        gate = jnp.dot(xin[...], gate_weight, preferred_element_type=F32).astype(BF)
        value = jnp.dot(xin[...], value_weight, preferred_element_type=F32).astype(BF)
        gate = rolled(gate.astype(F32), tg_ref[:, columns].astype(F32))
        value = rolled(value.astype(F32), tv_ref[:, columns].astype(F32))
        hid[:, columns] = (silu(gate) * value)[RIM:].astype(BF)

    chips = wall.shape[0] // blocks
    for n in range(blocks):
        down_weight = wall[n * chips : (n + 1) * chips, :, :, :, 2 * units :].reshape(512, units)
        part[:, n * 512 : (n + 1) * 512] = lax.dot_general(
            hid[...], down_weight, (((1,), (1,)), ((), ())), preferred_element_type=F32
        ).astype(BF)
    copies_q = []
    for k, dst in ((2, None), (1, q1), (3, q3), (0, q0)):
        first = pl.multiple_of(lax.rem(tp_index + k, 4) * share, 16)
        if dst is None:
            go(copies_q, part.at[pl.ds(first, share // 2)], q2a, sem_q)
            go(copies_q, part.at[pl.ds(first + share // 2, share // 2)], q2b, sem_q)
        else:
            go(copies_q, part.at[pl.ds(first, share)], dst, sem_q)
    for copy in copies_q:
        copy.wait()


def ffn(place, pieces, halo, residual, hres, out_weights, weights, gain, tg, tv):
    rows, width = residual.shape
    units = tg.shape[1]
    share = rows // 4
    hbm = pl.BlockSpec(memory_space=pl.ANY)
    vmem = pl.BlockSpec(memory_space=pltpu.VMEM)
    smem = pl.BlockSpec(memory_space=pltpu.SMEM)
    shape = jax.ShapeDtypeStruct
    return pl.pallas_call(
        ffn_kernel,
        in_specs=[smem] + [hbm] * 6 + [vmem] * 2 + [hbm] * 19 + [vmem] * 3,
        out_specs=[hbm] * 5 + [vmem],
        out_shape=[shape((share, width), BF)] * 3
        + [shape((share // 2, width), BF)] * 2
        + [shape((share, width), BF)],
        scratch_shapes=[
            pltpu.VMEM((rows + RIM, width), BF),
            pltpu.VMEM((width, width), BF),
            pltpu.VMEM((16, 2, 2, width // 64, 3 * units), BF),
            pltpu.VMEM((rows + RIM, width), BF),
            pltpu.VMEM((rows + RIM, width), BF),
            pltpu.VMEM((rows, units), BF),
            pltpu.VMEM((rows, width), BF),
            pltpu.SemaphoreType.DMA((9,)),
            pltpu.SemaphoreType.DMA((9,)),
            pltpu.SemaphoreType.DMA((32,)),
            pltpu.SemaphoreType.DMA((5,)),
        ],
        compiler_params=pltpu.CompilerParams(vmem_limit_bytes=60 * 1024 * 1024),
        name="ffn",
    )(place, *pieces, halo, residual, hres, *out_weights, *weights, gain, tg, tv)


def on_device(
    mixer_value_projection,
    write_vectors_projected,
    read_vectors_projected,
    output_gate_projected,
    step_size_scores,
    position_decay_extra,
    step_size_bias,
    head_decay_logarithm,
    value_filter_taps,
    write_filter_taps,
    read_filter_taps,
    gated_group_norm_gain,
    mixer_output_weight,
    residual,
    feedforward_norm_gain,
    feedforward_gate_weight,
    feedforward_value_weight,
    gate_filter_taps,
    single_value_filter_taps,
    feedforward_down_weight,
):
    row_count, inner = mixer_value_projection.shape
    core = lax.axis_index("sp_2")
    tp_index = lax.axis_index("tp")

    rows = jnp.concatenate(
        [feedforward_gate_weight, feedforward_value_weight, feedforward_down_weight.T], 1
    )
    part = rows.shape[0] // 2
    keep = jnp.where(core == 0, rows[:part], rows[part:])
    got = swapped(jnp.where(core == 0, rows[part:], rows[:part]))
    piece = jnp.concatenate([jnp.where(core == 0, keep, got), jnp.where(core == 0, got, keep)], 0)
    line = jnp.concatenate([piece, *turned_ring(piece, 0)], 0)
    plane = [line, *turned_ring(line, 1)]
    plane = [a.reshape(-1, 2, part, a.shape[1]) for a in plane]
    weights = [*plane, *named_swaps(plane)]

    own_half = lax.dynamic_slice_in_dim(mixer_output_weight, core * (inner // 2), inner // 2, 0)
    out_ring = gathered_ring(own_half, "tp")
    out_weights = [mixer_output_weight, *out_ring, *named_swaps(out_ring)]

    rim = jnp.concatenate(
        [
            a[row_count - RIM :]
            for a in (
                mixer_value_projection,
                write_vectors_projected,
                read_vectors_projected,
                residual,
            )
        ],
        1,
    )
    rim = shifted(rim, SP, 1)
    y, read, grow, packed = mixer_local(
        mixer_value_projection,
        write_vectors_projected,
        read_vectors_projected,
        rim[:, :inner],
        rim[:, inner : inner + STATE],
        rim[:, inner + STATE : inner + 2 * STATE],
        step_size_scores,
        position_decay_extra,
        step_size_bias[None],
        head_decay_logarithm[None],
        value_filter_taps,
        write_filter_taps,
        read_filter_taps,
    )
    state = state_before(packed)
    normed = mixer_finish(y, read, grow, output_gate_projected, state, gated_group_norm_gain[None])

    pieces = [normed, *gathered_ring(normed, "tp")]
    halo = shifted(normed[row_count - RIM :], SP, 1)
    halo = sent_to_all(halo, "tp")
    places = [lax.axis_index("sp_0"), lax.axis_index("sp_1"), core, tp_index]
    q0, q1, q3, q2a, q2b, own = ffn(
        jnp.stack(places).astype(jnp.int32),
        pieces,
        halo,
        residual,
        rim[:, inner + 2 * STATE :],
        out_weights,
        weights,
        feedforward_norm_gain[None],
        gate_filter_taps,
        single_value_filter_taps,
    )
    down = summed_ring(q0, q1, q3, q2a, q2b, "tp")
    return (own.astype(F32) + down).astype(BF)


def solution(mesh):
    torus = Mesh(mesh.devices.reshape(4, 4, 2, mesh.shape["tp"]), ("sp_0", "sp_1", "sp_2", "tp"))
    in_specs = (
        P(SP, "tp"),
        P(SP, "tp"),
        P(SP, "tp"),
        P(SP, "tp"),
        P(SP, "tp"),
        P(SP, "tp"),
        P("tp"),
        P("tp"),
        P(None, "tp"),
        P(None, "tp"),
        P(None, "tp"),
        P("tp"),
        P("tp", None),
        P(SP, None),
        P(),
        P(SP, "tp"),
        P(SP, "tp"),
        P(None, "tp"),
        P(None, "tp"),
        P("tp", SP),
    )
    out_specs = P(SP_TP, None)

    return jax.shard_map(
        on_device, mesh=torus, in_specs=in_specs, out_specs=out_specs, check_vma=False
    )
```

time: 347 us -> 252 us (0.73)
  blocking collectives: 90.5 us -> 0 us
  Pallas kernels: 0 us -> 58.2 us
  matrix products: 43.1 us -> 0 us
  starting transfers between devices: 21.6 us -> 60.5 us
  other arithmetic: 34.8 us -> 7.94 us
  between operations: 16.8 us -> 0.54 us
  local copies, waits for them, and re-layouts: 36.4 us -> 25.2 us
  waiting for transfers between devices: 102 us -> 96.5 us
    ppermute x5 -> x33, waiting for transfers between devices: 0.01 us -> 90.9 us  [the longest x14 73.6 us: shifted(): return lax.ppermute(value, axis, pairs)]
    reduce_scatter x1 -> x0, waiting for transfers between devices: 64.3 us -> none  [on_device(): lax.psum_scatter(jnp.dot(normed, mixer_output_weight, preferred_element_t...]
    pallas_call x0 -> x3, Pallas kernels: none -> 58.2 us  [the longest x1 40.8 us: ffn(): pl.pallas_call(ffn_kernel, in_specs=[smem] + [hbm] * 6 + [vmem] * 2 + [hb...]
    dot_general x8 -> x0, matrix products: 43.1 us -> none  [the longest x1 17.3 us: on_device(): jnp.dot(hidden, lax.all_gather(feedforward_down_weight, SP, axis=1, tiled...]
    all_to_all x1 -> x0, blocking collectives: 40.8 us -> none  [sent_and_summed(): parts = lax.all_to_all(split_up(value, dim, length), axis, 0, 0, tiled=True)]
    all_gather x4 -> x0, blocking collectives: 38.5 us -> none  [entering_2(): pieces = jax.tree.map(lambda part: lax.all_gather(part, axis), running)]
    all_to_all x1 -> x3, waiting for transfers between devices: 36.9 us -> 5.59 us  [sent_to_all(): lax.all_to_all(jnp.broadcast_to(value[None], (length, *value.shape)), axi...]
    ppermute x5 -> x33, starting transfers between devices: 16.8 us -> 47.4 us  [the longest x14 23.1 us: shifted(): return lax.ppermute(value, axis, pairs)]
  transfers between devices with their start and end apart: 9 -> 36, of which waited for: 2 -> 16; matrix products, arithmetic and copies ran while one was open for 16% -> 10% of each run, Pallas kernels for 0% -> 2%
where the time goes in v1:
time: 252 us; the launch traced here: 249 us
  waiting for transfers between devices  96.5 us (38%)
  starting transfers between devices  60.5 us (24%)
  Pallas kernels  58.2 us (23%)
  local copies, waits for them, and re-layouts  25.2 us (10%)
  other arithmetic  7.94 us (3%)
    ppermute x14, waiting for transfers between devices, shifted(): return lax.ppermute(value, axis, pairs)  73.6 us
    pallas_call x1, Pallas kernels, ffn(): pl.pallas_call(ffn_kernel, in_specs=[smem] + [hbm] * 6 + [vmem] * 2 + [hb...  40.8 us
    ppermute x14, starting transfers between devices, shifted(): return lax.ppermute(value, axis, pairs)  23.1 us
    ppermute x8, starting transfers between devices, turned(): return lax.ppermute(value, SP, pairs)  20.1 us
    ppermute x8, waiting for transfers between devices, turned(): return lax.ppermute(value, SP, pairs)  17.3 us
    all_to_all x3, starting transfers between devices, sent_to_all(): lax.all_to_all(jnp.broadcast_to(value[None], (length, *value.shape)), axi...  13.1 us
    pallas_call x1, Pallas kernels, mixer_local(): pl.pallas_call(mixer_kernel, grid=(rows // BLOCK,), in_specs=[by_block(in...  11.9 us
    unnamed x53, local copies, waits for them, and re-layouts  9.5 us
  transfers between devices with their start and end apart: 36, of which 16 were waited for; matrix products, arithmetic and copies ran while one was open for 10% of the time, Pallas kernels for 2%

profile of v1, /device:TPU:1, one launch (start us, length us, event | category | flops | bytes accessed | tf_op | source)
XLA Modules:
  0.0 248.8 jit_solution(14051630236611046598)
XLA Ops:
  3.9 4.6 %collective-permute-start = (bf16[16,2688]{1,0:T(8,128)(2,1)S(1)}, bf16[16,2688]{1,0:T(8,128)(2,1)S(1)}, u32[]{:S(2)}, u32[]{:S(2)}) collective-permute-start(bf16[16,2688]{1,0:T(8,128)(2,1)S(1)} %concatenate.37), channel_id=1, source_target_pairs={{0,4},{4,8},{8,12},{12,16},{16,20},{20,24},{24,28},{28,32},{32,36}... | collective-permute-start | bytes 258056 | tf_op jit(solution)/shard_map/ppermute | solution.py:29
  12.8 11.9 %mixer_local.1 = (f32[768,512]{1,0:T(8,128)}, bf16[768,64]{1,0:T(8,128)(2,1)}, f32[768,8]{1,0:T(8,128)}, bf16[80,512]{1,0:T(8,128)(2,1)}) custom-call(bf16[768,512]{1,0:T(8,128)(2,1)} %x_ref.1, bf16[768,64]{1,0:T(8,128)(2,1)} %copy-done.7, bf16[768,64]{1,0:T(8,128)(2,1)} %copy-done.8, bf16[16,512]{1,0:T(8,128)(2,1)} %slice.196.hx_ref, ...), custom_call_target="tpu_custom_call" | custom-call | tf_op jit(solution)/shard_map/mixer_local/pallas_call | solution.py:178
  27.1 4.0 %all-to-all-start = ((bf16[4,80,512]{2,1,0:T(8,128)(2,1)}), bf16[4,80,512]{2,1,0:T(8,128)(2,1)S(1)}, u32[]{:S(2)}, u32[]{:S(2)}) async-start(bf16[4,80,512]{2,1,0:T(8,128)(2,1)} %broadcast_in_dim.52), calls=%async_computation | async-start | bytes 655360 | tf_op jit(solution)/shard_map/all_to_all | solution.py:69
  33.5 4.6 %collective-permute-start.17 = (bf16[64,4224]{1,0:T(8,128)(2,1)}, bf16[64,4224]{1,0:T(8,128)(2,1)}, u32[]{:S(2)}, u32[]{:S(2)}) collective-permute-start(bf16[64,4224]{1,0:T(8,128)(2,1)} %pad_maximum_fusion.3), channel_id=1, source_target_pairs={{0,24},{4,100},{8,0},{12,108},{16,8},{20,116},{24,16},{28,124},{32... | collective-permute-start | bytes 1622024 | tf_op jit(solution)/shard_map/ppermute | solution.py:44
  39.1 5.8 %all-to-all-start.1 = ((bf16[4,80,512]{2,1,0:T(8,128)(2,1)}), bf16[4,80,512]{2,1,0:T(8,128)(2,1)S(1)}, u32[]{:S(2)}, u32[]{:S(2)}) async-start(bf16[4,80,512]{2,1,0:T(8,128)(2,1)} %broadcast_in_dim.54), calls=%async_computation.1 | async-start | bytes 655360 | tf_op jit(solution)/shard_map/all_to_all | solution.py:69
  46.0 2.5 collective-permute-start.8
  48.5 2.3 all-to-all-done.1
  54.5 1.9 constant_dynamic-update-slice_fusion.3
  56.4 1.9 constant_dynamic-update-slice_fusion.2
  58.3 2.6 %collective-permute-done.18 = bf16[32,4224]{1,0:T(8,128)(2,1)S(1)} collective-permute-done((bf16[32,4224]{1,0:T(8,128)(2,1)S(1)}, bf16[32,4224]{1,0:T(8,128)(2,1)S(1)}, u32[]{:S(2)}, u32[]{:S(2)}) %collective-permute-start.18) | collective-permute-done | bytes 270368 | tf_op jit(solution)/shard_map/ppermute | solution.py:44
  64.6 5.5 %mixer_finish.1.p0 = bf16[768,512]{1,0:T(8,128)(2,1)} custom-call(f32[768,512]{1,0:T(8,128)} %get-tuple-element.15.y_ref, bf16[768,64]{1,0:T(8,128)(2,1)} %get-tuple-element.16.read_ref, f32[768,8]{1,0:T(8,128)} %get-tuple-element.17.grow_ref, bf16[768,512]{1,0:T(8,128)(2,1)} %gate_ref.1, f32[64,512]{1,0:T(8,128)} %fusion.3.state_ref, f32[1,512]{1,0:T(1,128)} %bitcast.104), custom_call_target="tpu_custom_call" | custom-call | tf_op jit(solution)/shard_map/mixer_finish/pallas_call | solution.py:231
  70.8 5.3 %collective-permute-start.6 = (bf16[16,512]{1,0:T(8,128)(2,1)S(1)}, bf16[16,512]{1,0:T(8,128)(2,1)S(1)}, u32[]{:S(2)}, u32[]{:S(2)}) collective-permute-start(bf16[16,512]{1,0:T(8,128)(2,1)S(1)} %slice.221), channel_id=1, source_target_pairs={{0,4},{4,8},{8,12},{12,16},{16,20},{20,24},{24,28},{28,32},{32,36}... | collective-permute-start | bytes 49160 | tf_op jit(solution)/shard_map/ppermute | solution.py:29
  76.2 11.7 %collective-permute-done.6 = bf16[16,512]{1,0:T(8,128)(2,1)S(1)} collective-permute-done((bf16[16,512]{1,0:T(8,128)(2,1)S(1)}, bf16[16,512]{1,0:T(8,128)(2,1)S(1)}, u32[]{:S(2)}, u32[]{:S(2)}) %collective-permute-start.6) | collective-permute-done | bytes 16416 | tf_op jit(solution)/shard_map/ppermute | solution.py:29
  87.9 2.5 collective-permute-start.3
  91.5 2.7 %collective-permute-start.10 = (bf16[128,2048]{1,0:T(8,128)(2,1)S(1)}, bf16[128,2048]{1,0:T(8,128)(2,1)S(1)}, u32[]{:S(2)}, u32[]{:S(2)}) collective-permute-start(bf16[128,2048]{1,0:T(8,128)(2,1)S(1)} %slice.224), channel_id=1, source_target_pairs={{0,3},{1,0},{2,1},{3,2},{4,7},{5,4},{6,5},{7,6},{8,11},{9,8},{10,9... | collective-permute-start | bytes 1572872 | tf_op jit(solution)/shard_map/ppermute | solution.py:29
  95.3 8.3 %collective-permute-done.3.p2 = bf16[768,512]{1,0:T(8,128)(2,1)S(1)} collective-permute-done((bf16[768,512]{1,0:T(8,128)(2,1)}, bf16[768,512]{1,0:T(8,128)(2,1)S(1)}, u32[]{:S(2)}, u32[]{:S(2)}) %collective-permute-start.3) | collective-permute-done | bytes 786464 | tf_op jit(solution)/shard_map/ppermute | solution.py:29
  104.4 3.8 %collective-permute-done.2.p1 = bf16[768,512]{1,0:T(8,128)(2,1)S(1)} collective-permute-done((bf16[768,512]{1,0:T(8,128)(2,1)}, bf16[768,512]{1,0:T(8,128)(2,1)S(1)}, u32[]{:S(2)}, u32[]{:S(2)}) %collective-permute-start.2) | collective-permute-done | bytes 786464 | tf_op jit(solution)/shard_map/ppermute | solution.py:29
  109.2 4.7 %collective-permute-done.9.ofb = bf16[128,2048]{1,0:T(8,128)(2,1)S(1)} collective-permute-done((bf16[128,2048]{1,0:T(8,128)(2,1)S(1)}, bf16[128,2048]{1,0:T(8,128)(2,1)S(1)}, u32[]{:S(2)}, u32[]{:S(2)}) %collective-permute-start.9) | collective-permute-done | bytes 524320 | tf_op jit(solution)/shard_map/ppermute | solution.py:29
  114.7 7.6 %collective-permute-done.5.p3b = bf16[384,512]{1,0:T(8,128)(2,1)S(1)} collective-permute-done((bf16[384,512]{1,0:T(8,128)(2,1)S(1)}, bf16[384,512]{1,0:T(8,128)(2,1)S(1)}, u32[]{:S(2)}, u32[]{:S(2)}) %collective-permute-start.5) | collective-permute-done | bytes 393248 | tf_op jit(solution)/shard_map/ppermute | solution.py:29
  124.5 11.1 %collective-permute-done.4.p3a = bf16[384,512]{1,0:T(8,128)(2,1)S(1)} collective-permute-done((bf16[384,512]{1,0:T(8,128)(2,1)S(1)}, bf16[384,512]{1,0:T(8,128)(2,1)S(1)}, u32[]{:S(2)}, u32[]{:S(2)}) %collective-permute-start.4) | collective-permute-done | bytes 393248 | tf_op jit(solution)/shard_map/ppermute | solution.py:29
  136.3 12.4 %collective-permute-start.23 = (bf16[128,4224]{1,0:T(8,128)(2,1)S(1)}, bf16[128,4224]{1,0:T(8,128)(2,1)S(1)}, u32[]{:S(2)}, u32[]{:S(2)}) collective-permute-start(bf16[128,4224]{1,0:T(8,128)(2,1)S(1)} %slice.230), channel_id=1, source_target_pairs={{0,96},{4,28},{8,104},{12,4},{16,112},{20,12},{24,120},{28,20},{32... | collective-permute-start | bytes 3244040 | tf_op jit(solution)/shard_map/ppermute | solution.py:44
  149.8 11.0 %collective-permute-done.23 = bf16[128,4224]{1,0:T(8,128)(2,1)S(1)} collective-permute-done((bf16[128,4224]{1,0:T(8,128)(2,1)S(1)}, bf16[128,4224]{1,0:T(8,128)(2,1)S(1)}, u32[]{:S(2)}, u32[]{:S(2)}) %collective-permute-start.23) | collective-permute-done | bytes 1081376 | tf_op jit(solution)/shard_map/ppermute | solution.py:44
  160.7 3.7 %collective-permute-done.22 = bf16[128,4224]{1,0:T(8,128)(2,1)} collective-permute-done((bf16[128,4224]{1,0:T(8,128)(2,1)S(1)}, bf16[128,4224]{1,0:T(8,128)(2,1)}, u32[]{:S(2)}, u32[]{:S(2)}) %collective-permute-start.22) | collective-permute-done | bytes 1081376 | tf_op jit(solution)/shard_map/ppermute | solution.py:44
  166.4 3.3 %all-to-all-start.2 = ((bf16[4,16,512]{2,1,0:T(8,128)(2,1)}), bf16[4,16,512]{2,1,0:T(8,128)(2,1)S(1)}, u32[]{:S(2)}, u32[]{:S(2)}) async-start(bf16[4,16,512]{2,1,0:T(8,128)(2,1)} %broadcast_in_dim.58), calls=%async_computation.2 | async-start | bytes 131072 | tf_op jit(solution)/shard_map/all_to_all | solution.py:69
  171.0 3.2 %all-to-all-done.2.halo = bf16[4,16,512]{2,1,0:T(8,128)(2,1)S(1)} async-done(((bf16[4,16,512]{2,1,0:T(8,128)(2,1)}), bf16[4,16,512]{2,1,0:T(8,128)(2,1)S(1)}, u32[]{:S(2)}, u32[]{:S(2)}) %all-to-all-start.2) | async-done | bytes 65568 | tf_op jit(solution)/shard_map/all_to_all | solution.py:69
  174.8 40.8 %ffn.1 = (bf16[192,2048]{1,0:T(8,128)(2,1)}, bf16[192,2048]{1,0:T(8,128)(2,1)}, bf16[192,2048]{1,0:T(8,128)(2,1)}, bf16[96,2048]{1,0:T(8,128)(2,1)}, bf16[96,204...) custom-call(s32[4]{0:T(128)} %pad_add_fusion.place_ref, bf16[768,512]{1,0:T(8,128)(2,1)} %mixer_finish.1.p0, ...), custom_call_target="tpu_custom_call" | custom-call | tf_op jit(solution)/shard_map/ffn/pallas_call | solution.py:431
  219.3 6.1 %collective-permute-done.31 = bf16[96,2048]{1,0:T(8,128)(2,1)S(1)} collective-permute-done((bf16[96,2048]{1,0:T(8,128)(2,1)}, bf16[96,2048]{1,0:T(8,128)(2,1)S(1)}, u32[]{:S(2)}, u32[]{:S(2)}) %collective-permute-start.31) | collective-permute-done | bytes 393248 | tf_op jit(solution)/shard_map/ppermute | solution.py:29
  225.7 2.2 collective-permute-start.32
  227.8 1.4 collective-permute-done.29
  229.4 13.4 %collective-permute-done.32 = bf16[192,2048]{1,0:T(8,128)(2,1)S(1)} collective-permute-done((bf16[192,2048]{1,0:T(8,128)(2,1)S(1)}, bf16[192,2048]{1,0:T(8,128)(2,1)S(1)}, u32[]{:S(2)}, u32[]{:S(2)}) %collective-permute-start.32) | collective-permute-done | bytes 786464 | tf_op jit(solution)/shard_map/ppermute | solution.py:29
  242.8 4.6 %collective-permute-done.30 = bf16[192,2048]{1,0:T(8,128)(2,1)S(1)} collective-permute-done((bf16[192,2048]{1,0:T(8,128)(2,1)S(1)}, bf16[192,2048]{1,0:T(8,128)(2,1)S(1)}, u32[]{:S(2)}, u32[]{:S(2)}) %collective-permute-start.30) | collective-permute-done | bytes 786464 | tf_op jit(solution)/shard_map/ppermute | solution.py:29
  247.4 1.4 add_convert_fusion
  (148 shorter events, 39.5 us)
Async XLA Ops:
  27.1 11.1 %all-to-all-start = ((bf16[4,80,512]{2,1,0:T(8,128)(2,1)}), bf16[4,80,512]{2,1,0:T(8,128)(2,1)S(1)}, u32[]{:S(2)}, u32[]{:S(2)}) async-start(bf16[4,80,512]{2,1,0:T(8,128)(2,1)} %broadcast_in_dim.52), calls=%async_computation | async-start | bytes 655360 | tf_op jit(solution)/shard_map/all_to_all | solution.py:69
  33.5 17.3 %collective-permute-start.17 = (bf16[64,4224]{1,0:T(8,128)(2,1)}, bf16[64,4224]{1,0:T(8,128)(2,1)}, u32[]{:S(2)}, u32[]{:S(2)}) collective-permute-start(bf16[64,4224]{1,0:T(8,128)(2,1)} %pad_maximum_fusion.3), channel_id=1, source_target_pairs={{0,24},{4,100},{8,0},{12,108},{16,8},{20,116},{24,16},{28,124},{32... | collective-permute-start | bytes 1622024 | tf_op jit(solution)/shard_map/ppermute | solution.py:44
  38.2 14.8 %collective-permute-start.16 = (bf16[64,4224]{1,0:T(8,128)(2,1)}, bf16[64,4224]{1,0:T(8,128)(2,1)}, u32[]{:S(2)}, u32[]{:S(2)}) collective-permute-start(bf16[64,4224]{1,0:T(8,128)(2,1)} %pad_maximum_fusion.3), channel_id=1, source_target_pairs={{0,8},{4,36},{8,16},{12,44},{16,24},{20,52},{24,0},{28,60},{32,40}... | collective-permute-start | bytes 1622024 | tf_op jit(solution)/shard_map/ppermute | solution.py:44
  39.1 11.7 %all-to-all-start.1 = ((bf16[4,80,512]{2,1,0:T(8,128)(2,1)}), bf16[4,80,512]{2,1,0:T(8,128)(2,1)S(1)}, u32[]{:S(2)}, u32[]{:S(2)}) async-start(bf16[4,80,512]{2,1,0:T(8,128)(2,1)} %broadcast_in_dim.54), calls=%async_computation.1 | async-start | bytes 655360 | tf_op jit(solution)/shard_map/all_to_all | solution.py:69
  46.0 44.4 %collective-permute-start.8 = (bf16[256,2048]{1,0:T(8,128)(2,1)}, bf16[256,2048]{1,0:T(8,128)(2,1)}, u32[]{:S(2)}, u32[]{:S(2)}) collective-permute-start(bf16[256,2048]{1,0:T(8,128)(2,1)} %constant_dynamic-slice_fusion), channel_id=1, source_target_pairs={{0,3},{1,0},{2,1},{3,2},{4,7},{5,4},{6,5},{7,6},{8,11},{9,8},{10,9... | collective-permute-start | bytes 3145736 | tf_op jit(solution)/shard_map/ppermute | solution.py:29
  48.4 43.0 %collective-permute-start.7 = (bf16[256,2048]{1,0:T(8,128)(2,1)}, bf16[256,2048]{1,0:T(8,128)(2,1)}, u32[]{:S(2)}, u32[]{:S(2)}) collective-permute-start(bf16[256,2048]{1,0:T(8,128)(2,1)} %constant_dynamic-slice_fusion), channel_id=1, source_target_pairs={{0,1},{1,2},{2,3},{3,0},{4,5},{5,6},{6,7},{7,4},{8,9},{9,10},{10,1... | collective-permute-start | bytes 3145736 | tf_op jit(solution)/shard_map/ppermute | solution.py:29
  51.9 9.8 %collective-permute-start.19 = (bf16[32,4224]{1,0:T(8,128)(2,1)S(1)}, bf16[32,4224]{1,0:T(8,128)(2,1)S(1)}, u32[]{:S(2)}, u32[]{:S(2)}) collective-permute-start(bf16[32,4224]{1,0:T(8,128)(2,1)S(1)} %slice.228), channel_id=1, source_target_pairs={{0,24},{4,100},{8,0},{12,108},{16,8},{20,116},{24,16},{28,124},{32... | collective-permute-start | bytes 811016 | tf_op jit(solution)/shard_map/ppermute | solution.py:44
  62.3 59.9 %collective-permute-start.21 = (bf16[256,4224]{1,0:T(8,128)(2,1)}, bf16[256,4224]{1,0:T(8,128)(2,1)S(1)}, u32[]{:S(2)}, u32[]{:S(2)}) collective-permute-start(bf16[256,4224]{1,0:T(8,128)(2,1)} %constant_dynamic-update-slice_fusion), channel_id=1, source_target_pairs={{0,96},{4,28},{8,104},{12,4},{16,112},{20,12},{24,120},{28,20},{32... | collective-permute-start | bytes 6488072 | tf_op jit(solution)/shard_map/ppermute | solution.py:44
  63.5 59.4 %collective-permute-start.20 = (bf16[256,4224]{1,0:T(8,128)(2,1)}, bf16[256,4224]{1,0:T(8,128)(2,1)}, u32[]{:S(2)}, u32[]{:S(2)}) collective-permute-start(bf16[256,4224]{1,0:T(8,128)(2,1)} %constant_dynamic-update-slice_fusion), channel_id=1, source_target_pairs={{0,32},{4,12},{8,40},{12,20},{16,48},{20,28},{24,56},{28,4},{32,64... | collective-permute-start | bytes 6488072 | tf_op jit(solution)/shard_map/ppermute | solution.py:44
  70.8 17.0 %collective-permute-start.6 = (bf16[16,512]{1,0:T(8,128)(2,1)S(1)}, bf16[16,512]{1,0:T(8,128)(2,1)S(1)}, u32[]{:S(2)}, u32[]{:S(2)}) collective-permute-start(bf16[16,512]{1,0:T(8,128)(2,1)S(1)} %slice.221), channel_id=1, source_target_pairs={{0,4},{4,8},{8,12},{12,16},{16,20},{20,24},{24,28},{28,32},{32,36}... | collective-permute-start | bytes 49160 | tf_op jit(solution)/shard_map/ppermute | solution.py:29
  87.9 15.7 %collective-permute-start.3 = (bf16[768,512]{1,0:T(8,128)(2,1)}, bf16[768,512]{1,0:T(8,128)(2,1)S(1)}, u32[]{:S(2)}, u32[]{:S(2)}) collective-permute-start(bf16[768,512]{1,0:T(8,128)(2,1)} %mixer_finish.1.p0), channel_id=1, source_target_pairs={{0,3},{1,0},{2,1},{3,2},{4,7},{5,4},{6,5},{7,6},{8,11},{9,8},{10,9... | collective-permute-start | bytes 2359304 | tf_op jit(solution)/shard_map/ppermute | solution.py:29
  90.4 17.9 %collective-permute-start.2 = (bf16[768,512]{1,0:T(8,128)(2,1)}, bf16[768,512]{1,0:T(8,128)(2,1)S(1)}, u32[]{:S(2)}, u32[]{:S(2)}) collective-permute-start(bf16[768,512]{1,0:T(8,128)(2,1)} %mixer_finish.1.p0), channel_id=1, source_target_pairs={{0,1},{1,2},{2,3},{3,0},{4,5},{5,6},{6,7},{7,4},{8,9},{9,10},{10,1... | collective-permute-start | bytes 2359304 | tf_op jit(solution)/shard_map/ppermute | solution.py:29
  91.5 17.7 %collective-permute-start.10 = (bf16[128,2048]{1,0:T(8,128)(2,1)S(1)}, bf16[128,2048]{1,0:T(8,128)(2,1)S(1)}, u32[]{:S(2)}, u32[]{:S(2)}) collective-permute-start(bf16[128,2048]{1,0:T(8,128)(2,1)S(1)} %slice.224), channel_id=1, source_target_pairs={{0,3},{1,0},{2,1},{3,2},{4,7},{5,4},{6,5},{7,6},{8,11},{9,8},{10,9... | collective-permute-start | bytes 1572872 | tf_op jit(solution)/shard_map/ppermute | solution.py:29
  103.6 10.3 %collective-permute-start.9 = (bf16[128,2048]{1,0:T(8,128)(2,1)S(1)}, bf16[128,2048]{1,0:T(8,128)(2,1)S(1)}, u32[]{:S(2)}, u32[]{:S(2)}) collective-permute-start(bf16[128,2048]{1,0:T(8,128)(2,1)S(1)} %slice.223), channel_id=1, source_target_pairs={{0,1},{1,2},{2,3},{3,0},{4,5},{5,6},{6,7},{7,4},{8,9},{9,10},{10,1... | collective-permute-start | bytes 1572872 | tf_op jit(solution)/shard_map/ppermute | solution.py:29
  108.2 40.4 %collective-permute-start.12 = (bf16[256,2048]{1,0:T(8,128)(2,1)}, bf16[256,2048]{1,0:T(8,128)(2,1)S(1)}, u32[]{:S(2)}, u32[]{:S(2)}) collective-permute-start(bf16[256,2048]{1,0:T(8,128)(2,1)} %collective-permute-done.8.oa), channel_id=1, source_target_pairs={{0,4},{4,0},{1,5},{5,1},{2,6},{6,2},{3,7},{7,3},{8,12},{12,8},{9,1... | collective-permute-start | bytes 3145736 | tf_op jit(solution)/shard_map/ppermute | solution.py:33
  109.1 39.7 %collective-permute-start.11 = (bf16[256,2048]{1,0:T(8,128)(2,1)}, bf16[256,2048]{1,0:T(8,128)(2,1)S(1)}, u32[]{:S(2)}, u32[]{:S(2)}) collective-permute-start(bf16[256,2048]{1,0:T(8,128)(2,1)} %collective-permute-done.7.ob), channel_id=1, source_target_pairs={{0,4},{4,0},{1,5},{5,1},{2,6},{6,2},{3,7},{7,3},{8,12},{12,8},{9,1... | collective-permute-start | bytes 3145736 | tf_op jit(solution)/shard_map/ppermute | solution.py:33
  113.9 8.4 %collective-permute-start.5 = (bf16[384,512]{1,0:T(8,128)(2,1)S(1)}, bf16[384,512]{1,0:T(8,128)(2,1)S(1)}, u32[]{:S(2)}, u32[]{:S(2)}) collective-permute-start(bf16[384,512]{1,0:T(8,128)(2,1)S(1)} %slice.220), channel_id=1, source_target_pairs={{0,3},{1,0},{2,1},{3,2},{4,7},{5,4},{6,5},{7,6},{8,11},{9,8},{10,9... | collective-permute-start | bytes 1179656 | tf_op jit(solution)/shard_map/ppermute | solution.py:29
  122.3 14.0 %collective-permute-start.14 = (bf16[128,2048]{1,0:T(8,128)(2,1)S(1)}, bf16[128,2048]{1,0:T(8,128)(2,1)S(1)}, u32[]{:S(2)}, u32[]{:S(2)}) collective-permute-start(bf16[128,2048]{1,0:T(8,128)(2,1)S(1)} %collective-permute-done.10.ofa), channel_id=1, source_target_pairs={{0,4},{4,0},{1,5},{5,1},{2,6},{6,2},{3,7},{7,3},{8,12},{12,8},{9,1... | collective-permute-start | bytes 1572872 | tf_op jit(solution)/shard_map/ppermute | solution.py:33
  122.3 26.5 %collective-permute-start.13 = (bf16[128,2048]{1,0:T(8,128)(2,1)S(1)}, bf16[128,2048]{1,0:T(8,128)(2,1)S(1)}, u32[]{:S(2)}, u32[]{:S(2)}) collective-permute-start(bf16[128,2048]{1,0:T(8,128)(2,1)S(1)} %collective-permute-done.9.ofb), channel_id=1, source_target_pairs={{0,4},{4,0},{1,5},{5,1},{2,6},{6,2},{3,7},{7,3},{8,12},{12,8},{9,1... | collective-permute-start | bytes 1572872 | tf_op jit(solution)/shard_map/ppermute | solution.py:33
  123.1 12.5 %collective-permute-start.4 = (bf16[384,512]{1,0:T(8,128)(2,1)S(1)}, bf16[384,512]{1,0:T(8,128)(2,1)S(1)}, u32[]{:S(2)}, u32[]{:S(2)}) collective-permute-start(bf16[384,512]{1,0:T(8,128)(2,1)S(1)} %slice.219), channel_id=1, source_target_pairs={{0,1},{1,2},{2,3},{3,0},{4,5},{5,6},{6,7},{7,4},{8,9},{9,10},{10,1... | collective-permute-start | bytes 1179656 | tf_op jit(solution)/shard_map/ppermute | solution.py:29
  135.6 38.6 %collective-permute-start.24 = (bf16[4,2,32,4224]{3,2,1,0:T(8,128)(2,1)}, bf16[4,2,32,4224]{3,2,1,0:T(8,128)(2,1)}, u32[]{:S(2)}, u32[]{:S(2)}) collective-permute-start(bf16[4,2,32,4224]{3,2,1,0:T(8,128)(2,1)} %bitcast.29.w0), channel_id=1, source_target_pairs={{0,4},{4,0},{1,5},{5,1},{2,6},{6,2},{3,7},{7,3},{8,12},{12,8},{9,1... | collective-permute-start | bytes 6488072 | tf_op jit(solution)/shard_map/ppermute | solution.py:33
  136.3 24.5 %collective-permute-start.23 = (bf16[128,4224]{1,0:T(8,128)(2,1)S(1)}, bf16[128,4224]{1,0:T(8,128)(2,1)S(1)}, u32[]{:S(2)}, u32[]{:S(2)}) collective-permute-start(bf16[128,4224]{1,0:T(8,128)(2,1)S(1)} %slice.230), channel_id=1, source_target_pairs={{0,96},{4,28},{8,104},{12,4},{16,112},{20,12},{24,120},{28,20},{32... | collective-permute-start | bytes 3244040 | tf_op jit(solution)/shard_map/ppermute | solution.py:44
  148.7 25.5 %collective-permute-start.26 = (bf16[4,2,32,4224]{3,2,1,0:T(8,128)(2,1)S(1)}, bf16[4,2,32,4224]{3,2,1,0:T(8,128)(2,1)}, u32[]{:S(2)}, u32[]{:S(2)}) collective-permute-start(bf16[4,2,32,4224]{3,2,1,0:T(8,128)(2,1)S(1)} %bitcast.81), channel_id=1, source_target_pairs={{0,4},{4,0},{1,5},{5,1},{2,6},{6,2},{3,7},{7,3},{8,12},{12,8},{9,1... | collective-permute-start | bytes 6488072 | tf_op jit(solution)/shard_map/ppermute | solution.py:33
  148.8 15.7 %collective-permute-start.22 = (bf16[128,4224]{1,0:T(8,128)(2,1)S(1)}, bf16[128,4224]{1,0:T(8,128)(2,1)}, u32[]{:S(2)}, u32[]{:S(2)}) collective-permute-start(bf16[128,4224]{1,0:T(8,128)(2,1)S(1)} %slice.229), channel_id=1, source_target_pairs={{0,32},{4,12},{8,40},{12,20},{16,48},{20,28},{24,56},{28,4},{32,64... | collective-permute-start | bytes 3244040 | tf_op jit(solution)/shard_map/ppermute | solution.py:44
  148.9 25.3 %collective-permute-start.25 = (bf16[4,2,32,4224]{3,2,1,0:T(8,128)(2,1)}, bf16[4,2,32,4224]{3,2,1,0:T(8,128)(2,1)}, u32[]{:S(2)}, u32[]{:S(2)}) collective-permute-start(bf16[4,2,32,4224]{3,2,1,0:T(8,128)(2,1)} %bitcast.30.wb), channel_id=1, source_target_pairs={{0,4},{4,0},{1,5},{5,1},{2,6},{6,2},{3,7},{7,3},{8,12},{12,8},{9,1... | collective-permute-start | bytes 6488072 | tf_op jit(solution)/shard_map/ppermute | solution.py:33
  160.7 13.5 %collective-permute-start.28 = (bf16[2,2,32,4224]{3,2,1,0:T(8,128)(2,1)S(1)}, bf16[2,2,32,4224]{3,2,1,0:T(8,128)(2,1)}, u32[]{:S(2)}, u32[]{:S(2)}) collective-permute-start(bf16[2,2,32,4224]{3,2,1,0:T(8,128)(2,1)S(1)} %bitcast.83), channel_id=1, source_target_pairs={{0,4},{4,0},{1,5},{5,1},{2,6},{6,2},{3,7},{7,3},{8,12},{12,8},{9,1... | collective-permute-start | bytes 3244040 | tf_op jit(solution)/shard_map/ppermute | solution.py:33
  164.5 9.8 %collective-permute-start.27 = (bf16[2,2,32,4224]{3,2,1,0:T(8,128)(2,1)}, bf16[2,2,32,4224]{3,2,1,0:T(8,128)(2,1)}, u32[]{:S(2)}, u32[]{:S(2)}) collective-permute-start(bf16[2,2,32,4224]{3,2,1,0:T(8,128)(2,1)} %bitcast.32.wfb), channel_id=1, source_target_pairs={{0,4},{4,0},{1,5},{5,1},{2,6},{6,2},{3,7},{7,3},{8,12},{12,8},{9,1... | collective-permute-start | bytes 3244040 | tf_op jit(solution)/shard_map/ppermute | solution.py:33
  166.4 7.7 %all-to-all-start.2 = ((bf16[4,16,512]{2,1,0:T(8,128)(2,1)}), bf16[4,16,512]{2,1,0:T(8,128)(2,1)S(1)}, u32[]{:S(2)}, u32[]{:S(2)}) async-start(bf16[4,16,512]{2,1,0:T(8,128)(2,1)} %broadcast_in_dim.58), calls=%async_computation.2 | async-start | bytes 131072 | tf_op jit(solution)/shard_map/all_to_all | solution.py:69
  215.7 9.8 %collective-permute-start.31 = (bf16[96,2048]{1,0:T(8,128)(2,1)}, bf16[96,2048]{1,0:T(8,128)(2,1)S(1)}, u32[]{:S(2)}, u32[]{:S(2)}) collective-permute-start(bf16[96,2048]{1,0:T(8,128)(2,1)} %get-tuple-element.24), channel_id=1, source_target_pairs={{0,3},{1,0},{2,1},{3,2},{4,7},{5,4},{6,5},{7,6},{8,11},{9,8},{10,9... | collective-permute-start | bytes 1179656 | tf_op jit(solution)/shard_map/ppermute | solution.py:29
  218.7 10.5 %collective-permute-start.29 = (bf16[96,2048]{1,0:T(8,128)(2,1)S(1)}, bf16[96,2048]{1,0:T(8,128)(2,1)S(1)}, u32[]{:S(2)}, u32[]{:S(2)}) collective-permute-start(bf16[96,2048]{1,0:T(8,128)(2,1)S(1)} %copy-done.22), channel_id=1, source_target_pairs={{0,1},{1,2},{2,3},{3,0},{4,5},{5,6},{6,7},{7,4},{8,9},{9,10},{10,1... | collective-permute-start | bytes 1179656 | tf_op jit(solution)/shard_map/ppermute | solution.py:29
  225.7 17.2 %collective-permute-start.32 = (bf16[192,2048]{1,0:T(8,128)(2,1)S(1)}, bf16[192,2048]{1,0:T(8,128)(2,1)S(1)}, u32[]{:S(2)}, u32[]{:S(2)}) collective-permute-start(bf16[192,2048]{1,0:T(8,128)(2,1)S(1)} %pad_maximum_fusion.1), channel_id=1, source_target_pairs={{0,3},{1,0},{2,1},{3,2},{4,7},{5,4},{6,5},{7,6},{8,11},{9,8},{10,9... | collective-permute-start | bytes 2359304 | tf_op jit(solution)/shard_map/ppermute | solution.py:29
  229.4 18.1 %collective-permute-start.30 = (bf16[192,2048]{1,0:T(8,128)(2,1)S(1)}, bf16[192,2048]{1,0:T(8,128)(2,1)S(1)}, u32[]{:S(2)}, u32[]{:S(2)}) collective-permute-start(bf16[192,2048]{1,0:T(8,128)(2,1)S(1)} %pad_maximum_fusion), channel_id=1, source_target_pairs={{0,1},{1,2},{2,3},{3,0},{4,5},{5,6},{6,7},{7,4},{8,9},{9,10},{10,1... | collective-permute-start | bytes 2359304 | tf_op jit(solution)/shard_map/ppermute | solution.py:29
  (27 other events, 344.4 us)
